TPU v7x, 32 devices: a whole 2x2x4 slice. The times are simulated.
32 devices in a mesh: ep: 8 (over z, y), tp: 4 (over x, core).
Axes of the slice: x: 2, y: 2, z: 4, core: 2. Of those that a mesh axis runs over, the one named last changes fastest.
Arguments:
- tokens: bfloat16 [1024, 2048], P('ep'), may hold values from -6 to 6
- norm_gain: float32 [2048], replicated, may hold values from 0.1 to 1.9
- expert_ids: int32 [1024, 6], P('ep'), may hold values from 0 to 15, all different within a row; in each aligned block of 128 rows (0 to 127, 128 to 255, ...) at most 96 rows name the same one
- route_weights: float32 [1024, 6], P('ep'), may hold values from 0.1 to 1
- expert_gate: bfloat16 [32, 2048, 256], P(('ep', 'tp')), may hold values from -0.125 to 0.125
- expert_up: bfloat16 [32, 2048, 256], P(('ep', 'tp')), may hold values from -0.125 to 0.125
- expert_down: bfloat16 [32, 256, 2048], P(('ep', 'tp')), may hold values from -0.25 to 0.25
- shared_gate: bfloat16 [2048, 512], P(None, 'tp'), may hold values from -0.125 to 0.125
- shared_up: bfloat16 [2048, 512], P(None, 'tp'), may hold values from -0.125 to 0.125
- shared_down: bfloat16 [512, 2048], P(None, 'tp'), may hold values from -0.25 to 0.25
Outputs:
- mixed: bfloat16 [1024, 2048], P('ep', 'tp')
Inputs may be any that keep to these rules, and one draw needn't show every extreme that they name: `expert_ids`: each row names 6 different experts. In each aligned block of 128 rows (the rows of one index of ep) no expert is named by more than 96 rows, a bound that some block reaches.
All inputs are finite; a program needn't handle non-finite values.
Results may differ from a plain program's by a relative error of at most 0.0073.
Values may be sent and summed in bfloat16 or wider, within the bound.
A program may use at most 64 MiB of HBM per device.

v0:
```python
import jax
import jax.numpy as jnp
from jax import lax
from jax.sharding import PartitionSpec as P

NORM_EPSILON = 1e-06


def swapped(block, axis, distance):
    count = lax.axis_size(axis)
    route = []
    for low in range(count):
        high = low | 1 << distance
        if high != low and high < count:
            route += [(low, high), (high, low)]
    return lax.ppermute(block, axis, route)


def local(
    tokens,
    norm_gain,
    expert_ids,
    route_weights,
    expert_gate,
    expert_up,
    expert_down,
    shared_gate,
    shared_up,
    shared_down,
):
    ep_count = lax.axis_size("ep")
    tp_count = lax.axis_size("tp")
    pair_count = tp_count // 2
    tp_index = lax.axis_index("tp")
    column = tp_index // 2
    half_index = tp_index % 2
    token_count, model_width = tokens.shape
    top_count = expert_ids.shape[1]
    expert_count = ep_count * pair_count
    capacity = 2 * max(1, token_count * top_count // expert_count)
    half_cap = capacity // 2
    as_float = tokens.astype(jnp.float32)
    inverse_rms = lax.rsqrt(jnp.mean(as_float * as_float, axis=-1, keepdims=True) + NORM_EPSILON)
    normed = (as_float * inverse_rms * norm_gain).astype(jnp.bfloat16)
    expert_iota = jnp.arange(expert_count, dtype=jnp.int32)
    token_iota = jnp.arange(token_count, dtype=jnp.int32)
    counts = jnp.sum(
        (expert_ids[:, :, None] == expert_iota[None, None, :]).astype(jnp.bfloat16), axis=1
    )
    strict_lower = (token_iota[:, None] > token_iota[None, :]).astype(jnp.bfloat16)
    prefix = jnp.dot(strict_lower, counts, preferred_element_type=jnp.float32)
    slot_index = jnp.take_along_axis(prefix, expert_ids, axis=1).astype(jnp.int32)
    target = expert_ids // pair_count
    owner_column = expert_ids % pair_count
    is_mine = owner_column == column
    position = target * capacity + slot_index
    slot_iota = jnp.arange(ep_count * capacity, dtype=jnp.int32)
    matches = is_mine[None, :, :] & (position[None, :, :] == slot_iota[:, None, None])
    slot_taken = jnp.any(matches, axis=2)
    token_of_slot = jnp.sum(jnp.where(slot_taken, token_iota[None, :], 0), axis=1)
    filled = jnp.any(slot_taken, axis=1)
    buffer = jnp.where(
        filled[:, None], jnp.take(normed, token_of_slot, axis=0), jnp.zeros((), jnp.bfloat16)
    )
    buffer = buffer.reshape(ep_count, capacity, model_width)
    gate_local = expert_gate[0]
    up_local = expert_up[0]
    down_local = expert_down[0]
    received = lax.all_to_all(buffer, "ep", split_axis=0, concat_axis=0, tiled=True)
    flat_rows = received.reshape(-1, model_width)
    hidden = (
        jax.nn.silu(jnp.dot(flat_rows, gate_local, preferred_element_type=jnp.float32))
        * jnp.dot(flat_rows, up_local, preferred_element_type=jnp.float32)
    ).astype(jnp.bfloat16)
    partial_out = jnp.dot(hidden, down_local, preferred_element_type=jnp.float32).astype(
        jnp.bfloat16
    )
    partial_out = partial_out.reshape(received.shape[0], received.shape[1], model_width)
    kept_part = lax.dynamic_slice_in_dim(partial_out, half_index * half_cap, half_cap, 1)
    other_part = lax.dynamic_slice_in_dim(partial_out, (1 - half_index) * half_cap, half_cap, 1)
    partner_part = swapped(other_part, "tp", 0)
    expert_out = (kept_part.astype(jnp.float32) + partner_part.astype(jnp.float32)).astype(
        jnp.bfloat16
    )
    returned = lax.all_to_all(expert_out, "ep", split_axis=0, concat_axis=0, tiled=True)
    row_total = ep_count * half_cap
    flat_rows = returned.reshape(row_total, model_width).astype(jnp.float32)
    is_valid = is_mine & (slot_index // half_cap == half_index)
    row_index = jnp.where(is_valid, target * half_cap + slot_index % half_cap, -1)
    row_iota = jnp.arange(row_total, dtype=jnp.int32)
    hits = row_index[:, :, None] == row_iota[None, None, :]
    combine_table = jnp.sum(jnp.where(hits, route_weights[:, :, None], 0.0), axis=1)
    partial_routed = jnp.dot(
        combine_table,
        flat_rows,
        precision=lax.Precision.HIGHEST,
        preferred_element_type=jnp.float32,
    )
    routed = lax.psum_scatter(partial_routed, "tp", scatter_dimension=1, tiled=True)
    shared_act = (
        jax.nn.silu(jnp.dot(normed, shared_gate, preferred_element_type=jnp.float32))
        * jnp.dot(normed, shared_up, preferred_element_type=jnp.float32)
    ).astype(jnp.bfloat16)
    shared_out = jnp.dot(
        lax.all_gather(shared_act, "tp", axis=1, tiled=True),
        shared_down,
        preferred_element_type=jnp.float32,
    )
    return (routed + shared_out).astype(jnp.bfloat16)


def solution(mesh):
    return jax.shard_map(
        local,
        mesh=mesh,
        in_specs=(
            P("ep", None),
            P(),
            P("ep", None),
            P("ep", None),
            P(("ep", "tp"), None, None),
            P(("ep", "tp"), None, None),
            P(("ep", "tp"), None, None),
            P(None, "tp"),
            P(None, "tp"),
            P(None, "tp"),
        ),
        out_specs=P("ep", "tp"),
        check_vma=False,
    )
```

profile of v0, /device:TPU:0, one launch (start us, length us, event | category | flops | bytes accessed | tf_op | source)
XLA Modules:
  0.0 197.9 jit_solution(5964902168812083423)
XLA Ops:
  6.5 0.0 copy-start
  6.5 0.8 bitcast_or_fusion
  7.3 0.7 fusion.21
  8.0 0.7 fusion.22
  8.7 0.1 fusion.19
  8.9 0.1 copy.35
  9.0 0.1 reshape.75
  9.1 0.0 copy-start.3
  9.2 0.0 copy-start.1
  9.2 0.0 copy-start.4
  9.2 5.1 %gather_fusion.1 = f32[768]{0:T(1024)S(1)} fusion(f32[128,16]{0,1:T(8,128)S(1)} %fusion.19, s32[768]{0:T(1024)S(1)} %reshape.75), kind=kCustom, calls=%fused_computation.1 | custom fusion | bytes 12288 | tf_op jit(solution)/shard_map/jit(take_along_axis)/gather | solution.py:52
  14.3 0.1 reshape.78
  14.4 0.1 copy.36
  14.5 0.0 copy-done.3
  14.6 0.4 fusion.2
  15.0 0.2 select_reduce_fusion.1
  15.2 0.1 reduce_sum.46
  15.3 0.0 copy-done.1
  15.3 0.2 fusion.5
  15.5 0.1 broadcast_in_dim.71
  15.6 0.0 copy-done.4
  15.6 0.2 fusion.7
  15.8 4.3 %gather_fusion = bf16[768,2048]{1,0:T(8,128)(2,1)} fusion(bf16[128,2048]{1,0:T(8,128)(2,1)S(1)} %fusion.7, s32[1024]{0:T(1024)S(1)} %pad_clamp_fusion), kind=kCustom, calls=%fused_computation | custom fusion | bytes 6294528 | tf_op jit(solution)/shard_map/jit(_take)/gather | solution.py:63
  20.1 3.3 %select_select_fusion = bf16[8,96,2048]{2,1,0:T(8,128)(2,1)} fusion(bf16[8,96,2048]{2,1,0:T(8,128)(2,1)} %bitcast.29, pred[8,96]{1,0:T(8,128)(4,1)S(1)} %compare_and_fusion, pred[8,96]{1,0:T(8,128)(4,1)S(1)} %broadcast_in_dim.71), kind=kLoop, calls=%fused_computation.4 | loop fusion | flops 3145728 | bytes 6292992 | tf_op jit(solution)/shard_map/jit(_where)/select_n | solution.py:62
  23.4 7.4 %all-to-all-start = ((bf16[8,96,2048]{2,1,0:T(8,128)(2,1)}), bf16[8,96,2048]{2,1,0:T(8,128)(2,1)}, u32[]{:S(2)}, u32[]{:S(2)}) async-start(bf16[8,96,2048]{2,1,0:T(8,128)(2,1)} %select_select_fusion), calls=%async_computation | async-start | bytes 6291456 | tf_op jit(solution)/shard_map/all_to_all | solution.py:69
  30.9 70.8 %all-to-all-done = bf16[8,96,2048]{2,1,0:T(8,128)(2,1)} async-done(((bf16[8,96,2048]{2,1,0:T(8,128)(2,1)}), bf16[8,96,2048]{2,1,0:T(8,128)(2,1)}, u32[]{:S(2)}, u32[]{:S(2)}) %all-to-all-start) | async-done | bytes 3145760 | tf_op jit(solution)/shard_map/all_to_all | solution.py:69
  101.7 0.0 copy-done.6
  101.7 3.8 %fusion.11 = f32[768,256]{1,0:T(8,128)} fusion(bf16[768,2048]{1,0:T(8,128)(2,1)} %bitcast.2, bf16[1,2048,256]{2,1,0:T(8,128)(2,1)S(1)} %copy-done.6), kind=kOutput, calls=%fused_computation.22 | convolution fusion | flops 805306368 | bytes 4980736 | tf_op jit(solution)/shard_map/dot_general | solution.py:72
  105.4 0.0 copy-done
  105.4 7.4 %convolution_convert_fusion = bf16[768,2048]{1,0:T(8,128)(2,1)} fusion(bf16[768,2048]{1,0:T(8,128)(2,1)} %bitcast.2, bf16[1,256,2048]{2,1,0:T(8,128)(2,1)S(1)} %copy-done, bf16[1,2048,256]{2,1,0:T(8,128)(2,1)} %param.15, f32[768,256]{1,0:T(8,128)} %fusion.11), kind=kOutput, calls=%fused_computation.2 | convolution fusion | flops 1613365248 | bytes 9175040 | tf_op jit(solution)/shard_map/dot_general | solution.py:75
  112.8 2.7 %constant_dynamic-slice_fusion = bf16[8,48,2048]{2,1,0:T(8,128)(2,1)} fusion(bf16[8,96,2048]{2,1,0:T(8,128)(2,1)} %bitcast.31, s32[]{:T(128)S(6)} %select_n.98), kind=kLoop, calls=%fused_computation.64 | loop fusion | bytes 3145732 | tf_op jit(solution)/shard_map/dynamic_slice | solution.py:80
  115.5 0.0 collective-permute-start
  115.5 3.6 %collective-permute-done = bf16[8,48,2048]{2,1,0:T(8,128)(2,1)S(1)} collective-permute-done((bf16[8,48,2048]{2,1,0:T(8,128)(2,1)}, bf16[8,48,2048]{2,1,0:T(8,128)(2,1)S(1)}, u32[]{:S(2)}, u32[]{:S(2)}) %collective-permute-start) | collective-permute-done | bytes 1572896 | tf_op jit(solution)/shard_map/ppermute | solution.py:16
  119.2 3.2 %add_convert_fusion = bf16[8,48,2048]{2,1,0:T(8,128)(2,1)} fusion(bf16[8,48,2048]{2,1,0:T(8,128)(2,1)S(1)} %collective-permute-done, bf16[8,96,2048]{2,1,0:T(8,128)(2,1)} %bitcast.32, s32[]{:T(128)S(6)} %select_n.97), kind=kLoop, calls=%fused_computation.3 | loop fusion | flops 3145728 | bytes 4718596 | tf_op jit(solution)/shard_map/convert_element_type | solution.py:82
  122.3 3.6 %all-to-all-start.1 = ((bf16[8,48,2048]{2,1,0:T(8,128)(2,1)}), bf16[8,48,2048]{2,1,0:T(8,128)(2,1)S(1)}, u32[]{:S(2)}, u32[]{:S(2)}) async-start(bf16[8,48,2048]{2,1,0:T(8,128)(2,1)} %add_convert_fusion), calls=%async_computation.1 | async-start | bytes 3145728 | tf_op jit(solution)/shard_map/all_to_all | solution.py:85
  126.0 0.0 reduce-scatter.2.cloned.1.call-start
  126.0 0.0 copy-done.5
  126.0 0.3 select_reduce_fusion
  126.3 37.1 %all-to-all-done.1 = bf16[8,48,2048]{2,1,0:T(8,128)(2,1)S(1)} async-done(((bf16[8,48,2048]{2,1,0:T(8,128)(2,1)}), bf16[8,48,2048]{2,1,0:T(8,128)(2,1)S(1)}, u32[]{:S(2)}, u32[]{:S(2)}) %all-to-all-start.1) | async-done | bytes 1572896 | tf_op jit(solution)/shard_map/all_to_all | solution.py:85
  163.4 2.0 fusion.31
  165.4 0.0 reduce-scatter.2.cloned.1.call-update
  165.4 1.4 fusion.32
  166.8 1.3 fusion.4
  168.1 5.4 %all_gather.3 = bf16[128,512]{1,0:T(8,128)(2,1)S(1)} all-gather(bf16[128,128]{1,0:T(8,128)(2,1)S(1)} %fusion.4), channel_id=1, replica_groups=mesh['ep'=8,'tp'=4] {'tp'}, dimensions={1}, use_global_device_ids=true | all-gather | bytes 163840 | tf_op jit(solution)/shard_map/all_gather | solution.py:105
  173.6 0.0 copy-done.2
  173.6 0.2 fusion.33
  173.8 15.6 %reduce-scatter.2.cloned.1.call-done = f32[128,512]{1,0:T(8,128)} async-done(((f32[128,2048]{1,0:T(8,128)}), f32[128,512]{1,0:T(8,128)}) %reduce-scatter.2.cloned.1.call-update) | async-done | bytes 262160 | tf_op jit(solution)/shard_map/reduce_scatter | solution.py:99
  189.4 1.6 add_convert_fusion.1
  (8 shorter events, 0.1 us)
Async XLA Ops:
  6.5 98.9 %copy-start = (bf16[1,256,2048]{2,1,0:T(8,128)(2,1)S(1)}, bf16[1,256,2048]{2,1,0:T(8,128)(2,1)}, u32[]{:S(2)}) copy-start(bf16[1,256,2048]{2,1,0:T(8,128)(2,1)} %param.16) | copy-start | bytes 3145732
  9.1 5.4 %copy-start.3 = (s32[128,6]{0,1:T(8,128)S(1)}, s32[128,6]{0,1:T(8,128)}, u32[]{:S(2)}) copy-start(s32[128,6]{0,1:T(8,128)} %param.12) | copy-start | bytes 9220
  9.2 6.1 %copy-start.1 = (bf16[128,2048]{1,0:T(8,128)(2,1)S(1)}, bf16[128,2048]{1,0:T(8,128)(2,1)}, u32[]{:S(2)}) copy-start(bf16[128,2048]{1,0:T(8,128)(2,1)} %param.10) | copy-start | bytes 1572868
  9.2 6.4 %copy-start.4 = (f32[2048]{0:T(1024)S(1)}, f32[2048]{0:T(1024)}, u32[]{:S(2)}) copy-start(f32[2048]{0:T(1024)} %param.11) | copy-start | bytes 24580
  23.4 78.3 %copy-start.6 = (bf16[1,2048,256]{2,1,0:T(8,128)(2,1)S(1)}, bf16[1,2048,256]{2,1,0:T(8,128)(2,1)}, u32[]{:S(2)}) copy-start(bf16[1,2048,256]{2,1,0:T(8,128)(2,1)} %param.14) | copy-start | bytes 3145732
  23.4 78.3 %all-to-all-start = ((bf16[8,96,2048]{2,1,0:T(8,128)(2,1)}), bf16[8,96,2048]{2,1,0:T(8,128)(2,1)}, u32[]{:S(2)}, u32[]{:S(2)}) async-start(bf16[8,96,2048]{2,1,0:T(8,128)(2,1)} %select_select_fusion), calls=%async_computation | async-start | bytes 6291456 | tf_op jit(solution)/shard_map/all_to_all | solution.py:69
  115.5 3.6 %collective-permute-start = (bf16[8,48,2048]{2,1,0:T(8,128)(2,1)}, bf16[8,48,2048]{2,1,0:T(8,128)(2,1)S(1)}, u32[]{:S(2)}, u32[]{:S(2)}) collective-permute-start(bf16[8,48,2048]{2,1,0:T(8,128)(2,1)} %constant_dynamic-slice_fusion), channel_id=1, source_target_pairs={{0,1},{1,0},{2,3},{3,2},{4,5},{5,4},{6,7},{7,6},{8,9},{9,8},{10,11... | collective-permute-start | bytes 4718600 | tf_op jit(solution)/shard_map/ppermute | solution.py:16
  115.5 10.5 %copy-start.5 = (f32[128,6]{0,1:T(8,128)S(1)}, f32[128,6]{0,1:T(8,128)}, u32[]{:S(2)}) copy-start(f32[128,6]{0,1:T(8,128)} %param.13) | copy-start | bytes 9220
  122.3 41.1 %all-to-all-start.1 = ((bf16[8,48,2048]{2,1,0:T(8,128)(2,1)}), bf16[8,48,2048]{2,1,0:T(8,128)(2,1)S(1)}, u32[]{:S(2)}, u32[]{:S(2)}) async-start(bf16[8,48,2048]{2,1,0:T(8,128)(2,1)} %add_convert_fusion), calls=%async_computation.1 | async-start | bytes 3145728 | tf_op jit(solution)/shard_map/all_to_all | solution.py:85
  126.0 63.5 %reduce-scatter.2.cloned.1.call-start = ((), (), s32[]{:S(2)}) async-start(), calls=%async_computation.3 | async-start | bytes 1310720 | tf_op jit(solution)/shard_map/reduce_scatter | solution.py:99
  165.4 8.2 %copy-start.2 = (bf16[512,512]{1,0:T(8,128)(2,1)S(1)}, bf16[512,512]{1,0:T(8,128)(2,1)}, u32[]{:S(2)}) copy-start(bf16[512,512]{1,0:T(8,128)(2,1)} %param.19) | copy-start | bytes 1572868
Sparse Core Ops, SparseCore 0:
  165.5 23.8 reduce-scatter.1
where the time goes:
time: 198 us
  waiting for transfers between devices  127 us (64%)
  matrix products  16.2 us (8%)
  between operations  13.6 us (7%)
  local copies, waits for them, and re-layouts  12.8 us (6%)
  other arithmetic  11.6 us (6%)
  starting transfers between devices  11.1 us (6%)
  blocking collectives  5.45 us (3%)
    all_to_all x1, waiting for transfers between devices, local(): lax.all_to_all(buffer, 'ep', split_axis=0, concat_axis=0, tiled=True)  70.8 us
    all_to_all x1, waiting for transfers between devices, local(): lax.all_to_all(expert_out, 'ep', split_axis=0, concat_axis=0, tiled=True)  37.1 us
    reduce_scatter x1, waiting for transfers between devices, local(): lax.psum_scatter(partial_routed, 'tp', scatter_dimension=1, tiled=True)  15.6 us
    all_to_all x1, starting transfers between devices, local(): lax.all_to_all(buffer, 'ep', split_axis=0, concat_axis=0, tiled=True)  7.44 us
    dot_general x1, matrix products, local(): jnp.dot(hidden, down_local, preferred_element_type=jnp.float32)  7.39 us
    gather x5, local copies, waits for them, and re-layouts, local(): jnp.take_along_axis(prefix, expert_ids, axis=1).astype(jnp.int32)  5.56 us
    all_gather x1, blocking collectives, local(): lax.all_gather(shared_act, 'tp', axis=1, tiled=True)  5.45 us
    gather x1, local copies, waits for them, and re-layouts, local(): jnp.take(normed, token_of_slot, axis=0)  4.29 us
  transfers between devices with their start and end apart: 4, of which 4 were waited for; matrix products, arithmetic and copies ran while one was open for 2% of the time, Pallas kernels for 0%

commit v1 on v0

--- a/solution.py
+++ b/solution.py
@@ -1,6 +1,10 @@
+import functools
+
 import jax
 import jax.numpy as jnp
 from jax import lax
+from jax.experimental import pallas as pl
+from jax.experimental.pallas import tpu as pltpu
 from jax.sharding import PartitionSpec as P
 
 NORM_EPSILON = 1e-06
@@ -16,7 +20,7 @@
     return lax.ppermute(block, axis, route)
 
 
-def local(
+def routed_exchange(
     tokens,
     norm_gain,
     expert_ids,
@@ -109,6 +113,421 @@
     return (routed + shared_out).astype(jnp.bfloat16)
 
 
+MESH = pl.DeviceIdType.MESH
+LANES = 128
+
+
+def silu(v):
+    return v / (1.0 + jnp.exp(-v))
+
+
+def dense_kernel(
+    ep_count, tp_count, minor, split,
+    tok_ref, gain_ref, wt_ref, gate_hbm, up_hbm, down_hbm, sg_hbm, su_hbm, sd_hbm,
+    out_ref,
+    x_buf, y_buf, c_buf, xs_buf, xr_buf, zs_buf, zr_buf, ys_buf, yr_buf, fs_buf, fr_buf,
+    acc, wt_all, sh_all, sh_out, gate, up, down, sg, su, sd,
+    load_sem, wt_s, wt_r, sh_s, sh_r, y_s, u_s, d_s, z_r, x_s, x_r, c_s, c_r,
+    yc_s, yc_r, rx_s, rx_r, rz_s, rz_r, ry_s, ry_r, f_s, f_r,
+):
+    major = ep_count // minor
+    rows = tok_ref.shape[0]
+    quarter = x_buf.shape[3]
+    e = lax.axis_index("ep")
+    t = lax.axis_index("tp")
+    z = e // minor
+    y = e % minor
+    xi = t // 2
+    c = t % 2
+    t2 = 2 * (1 - xi) + c
+    mate_x = {"tp": t2}
+    mate_c = {"tp": 2 * xi + 1 - c}
+    mate_y = {"ep": z * minor + 1 - y}
+    z_up = {"ep": lax.rem(e + minor, ep_count)}
+    z_down = {"ep": lax.rem(e + ep_count - minor, ep_count)}
+    head_cols = pl.ds(0, split)
+    rest_cols = pl.ds(split, quarter - split)
+
+    def remote(src, dst, s, r, who):
+        return pltpu.make_async_remote_copy(
+            src_ref=src, dst_ref=dst, send_sem=s, recv_sem=r, device_id=who, device_id_type=MESH
+        )
+
+    loads = [
+        pltpu.make_async_copy(a, b, load_sem.at[i])
+        for i, (a, b) in enumerate(
+            ((sg_hbm, sg), (su_hbm, su), (gate_hbm, gate), (up_hbm, up), (down_hbm, down), (sd_hbm, sd))
+        )
+    ]
+    for load in loads:
+        load.start()
+
+    barrier = pltpu.get_barrier_semaphore()
+    for k in range(1, ep_count):
+        pl.semaphore_signal(barrier, inc=1, device_id={"ep": lax.rem(e + k, ep_count)}, device_id_type=MESH)
+    for k in range(1, tp_count):
+        pl.semaphore_signal(barrier, inc=1, device_id={"tp": lax.rem(t + k, tp_count)}, device_id_type=MESH)
+
+    step = 16
+
+    def norm_rows(i, carry):
+        part = pl.ds(pl.multiple_of(i * step, step), step)
+        v = tok_ref[part, :].astype(jnp.float32)
+        r = lax.rsqrt(jnp.mean(v * v, axis=-1, keepdims=True) + NORM_EPSILON)
+        n = (v * r * gain_ref[...]).astype(jnp.bfloat16)
+        for q in range(tp_count):
+            x_buf[e, q, part, :] = n[:, q * quarter : (q + 1) * quarter]
+        return carry
+
+    lax.fori_loop(0, rows // step, norm_rows, 0)
+    pl.semaphore_wait(barrier, ep_count + tp_count - 2)
+
+    def wt_copy(k, slot, who):
+        src = wt_ref if slot is None else wt_all.at[slot]
+        dst = wt_all.at[e if slot is None else slot]
+        return remote(src, dst, wt_s.at[k], wt_r.at[k], {"ep": who})
+
+    def main_of(g):
+        return x_buf.at[g, t]
+
+    def rest_of(g):
+        return x_buf.at[g, t2, :, rest_cols]
+
+    def line(g, s, who):
+        return (
+            remote(main_of(g), main_of(g), s.at[g, 0], z_r.at[g, 0], who),
+            remote(rest_of(g), rest_of(g), s.at[g, 1], z_r.at[g, 1], who),
+        )
+
+    def x_copy(g):
+        ref = x_buf.at[g, t, :, head_cols]
+        return remote(ref, ref, x_s.at[g], x_r.at[g], mate_x)
+
+    def x_arrival(g):
+        ref = x_buf.at[g, t2, :, head_cols]
+        return remote(ref, ref, x_s.at[g], x_r.at[g], mate_x)
+
+    def c_copies(g, lane):
+        main, other = 2 * xi + lane, 2 * (1 - xi) + lane
+        refs = (x_buf.at[g, main], x_buf.at[g, other, :, rest_cols], x_buf.at[g, other, :, head_cols])
+        return [remote(r, r, c_s.at[g, i], c_r.at[g, i], mate_c) for i, r in enumerate(refs)]
+
+    def order(j):
+        k = jnp.minimum(z, major - 1 - z)
+        d = (j + 1) // 2
+        near = jnp.where(j % 2 == 1, z - d, z + d)
+        far = jnp.where(z <= major - 1 - z, j, major - 1 - j)
+        return jnp.where(j <= 2 * k, near, far)
+
+    def slot_group(i):
+        p = order(i // 2)
+        yy = jnp.where(i % 2 == 0, y, 1 - y)
+        return p, p * minor + yy
+
+    def forward(p, g):
+        @pl.when((p <= z) & (z < major - 1))
+        def _():
+            for copy in line(g, u_s, z_up):
+                copy.start()
+
+        @pl.when((p >= z) & (z > 0))
+        def _():
+            for copy in line(g, d_s, z_down):
+                copy.start()
+
+    for copy in line(e, y_s, mate_y):
+        copy.start()
+    for k in range(1, ep_count):
+        wt_copy(k, None, lax.rem(e + k, ep_count)).start()
+    wt_all[e] = wt_ref[...]
+    forward(z, e)
+
+    loads[0].wait()
+    loads[1].wait()
+    sg_sum = jnp.zeros((rows, sg.shape[1]), jnp.float32)
+    su_sum = jnp.zeros((rows, sg.shape[1]), jnp.float32)
+    for q in range(tp_count):
+        band = pl.ds(q * quarter, quarter)
+        sg_sum += jnp.dot(x_buf[e, q], sg[band, :], preferred_element_type=jnp.float32)
+        su_sum += jnp.dot(x_buf[e, q], su[band, :], preferred_element_type=jnp.float32)
+    sh_all[t] = (silu(sg_sum) * su_sum).astype(jnp.bfloat16)
+
+    def sh_copy(k, slot, who):
+        return remote(sh_all.at[slot], sh_all.at[slot], sh_s.at[k], sh_r.at[k], {"tp": who})
+
+    for k in range(1, tp_count):
+        sh_copy(k, t, lax.rem(t + k, tp_count)).start()
+    for load in loads[2:5]:
+        load.wait()
+    for k in range(1, ep_count):
+        wt_copy(k, lax.rem(e + ep_count - k, ep_count), e).wait_recv()
+
+    expert = e * (tp_count // 2) + xi
+    expert_mask = lax.broadcasted_iota(jnp.int32, wt_ref.shape, 0) == expert
+    eye = lax.broadcasted_iota(jnp.int32, (rows, rows), 0) == lax.broadcasted_iota(
+        jnp.int32, (rows, rows), 1
+    )
+
+    def compute(g):
+        row = jnp.sum(jnp.where(expert_mask, wt_all[g], 0.0), axis=0, keepdims=True)
+        weight = jnp.sum(jnp.where(eye, row, 0.0), axis=1, keepdims=True)
+        ff = gate.shape[1]
+        g_sum = jnp.zeros((rows, ff), jnp.float32)
+        u_sum = jnp.zeros((rows, ff), jnp.float32)
+        for q in range(tp_count):
+            band = pl.ds(q * quarter, quarter)
+            g_sum += jnp.dot(x_buf[g, q], gate[band, :], preferred_element_type=jnp.float32)
+            u_sum += jnp.dot(x_buf[g, q], up[band, :], preferred_element_type=jnp.float32)
+        act = (silu(g_sum) * u_sum).astype(jnp.bfloat16)
+        for q in range(tp_count):
+            part = jnp.dot(
+                act, down[:, q * quarter : (q + 1) * quarter], preferred_element_type=jnp.float32
+            )
+            y_buf[g, q] = (part * weight).astype(jnp.bfloat16)
+
+    def yc_copy(g, k):
+        return remote(
+            y_buf.at[g, 2 * k + 1 - c], c_buf.at[g, k], yc_s.at[g, k], yc_r.at[g, k], mate_c
+        )
+
+    def rx_copy(g):
+        return remote(xs_buf.at[g], xr_buf.at[g], rx_s.at[g], rx_r.at[g], mate_x)
+
+    total = ep_count
+
+    def main_step(i, carry):
+        @pl.when((i >= 1) & (i < total))
+        def _():
+            p, g = slot_group(i)
+            for copy in line(g, u_s, z_up):
+                copy.wait_recv()
+            forward(p, g)
+            x_copy(g).start()
+            ours = c_copies(g, c)
+            ours[0].start()
+            ours[1].start()
+
+        @pl.when((i >= 1) & (i <= total))
+        def _():
+            _, g = slot_group(i - 1)
+
+            @pl.when(i >= 2)
+            def _():
+                x_arrival(g).wait_recv()
+                c_copies(g, c)[2].start()
+                for copy in c_copies(g, 1 - c):
+                    copy.wait_recv()
+
+            compute(g)
+            for k in range(2):
+                yc_copy(g, k).start()
+
+        @pl.when(i >= 2)
+        def _():
+            _, g = slot_group(i - 2)
+            for k in range(2):
+                yc_copy(g, k).wait_recv()
+            xs_buf[g] = (
+                y_buf[g, t2, :, head_cols].astype(jnp.float32)
+                + c_buf[g, 1 - xi, :, head_cols].astype(jnp.float32)
+            ).astype(jnp.bfloat16)
+            rx_copy(g).start()
+
+        return carry
+
+    lax.fori_loop(0, total + 2, main_step, 0)
+
+    loads[5].wait()
+    for k in range(1, tp_count):
+        sh_copy(k, lax.rem(t + tp_count - k, tp_count), t).wait_recv()
+    shared = jnp.zeros((rows, quarter), jnp.float32)
+    width = sg.shape[1]
+    for q in range(tp_count):
+        shared += jnp.dot(
+            sh_all[q], sd[q * width : (q + 1) * width, :], preferred_element_type=jnp.float32
+        )
+    sh_out[...] = shared
+
+    def rz_copy(g, lane, who):
+        return remote(zs_buf.at[g], zr_buf.at[lane, g], rz_s.at[g], rz_r.at[lane, g], who)
+
+    def gather_sum(p, g):
+        rx_copy(g).wait_recv()
+        mine = y_buf[g, t].astype(jnp.float32) + c_buf[g, xi].astype(jnp.float32)
+        acc[:, :split] = mine[:, :split] + xr_buf[g].astype(jnp.float32)
+        acc[:, split:quarter] = mine[:, split:]
+        acc[:, quarter:] = y_buf[g, t2, :, rest_cols].astype(jnp.float32) + c_buf[
+            g, 1 - xi, :, rest_cols
+        ].astype(jnp.float32)
+
+        @pl.when((p >= z) & (z > 0))
+        def _():
+            rz_copy(g, 0, z_up).wait_recv()
+            acc[...] += zr_buf[0, g].astype(jnp.float32)
+
+        @pl.when((p <= z) & (z < major - 1))
+        def _():
+            rz_copy(g, 1, z_up).wait_recv()
+            acc[...] += zr_buf[1, g].astype(jnp.float32)
+
+    def sum_step(i, carry):
+        q = i // 2
+        ups = major - 1 - z
+        low = jnp.where(q < ups, z + 1 + q, z - 1 - (q - ups))
+        high = jnp.where(q < z, z - 1 - q, z + 1 + (q - z))
+        p = jnp.where(2 * z < major, low, high)
+        g = p * minor + jnp.where(i % 2 == 0, y, 1 - y)
+        gather_sum(p, g)
+        zs_buf[g] = acc[...].astype(jnp.bfloat16)
+
+        @pl.when(p > z)
+        def _():
+            rz_copy(g, 0, z_up).start()
+
+        @pl.when(p < z)
+        def _():
+            rz_copy(g, 1, z_down).start()
+
+        return carry
+
+    lax.fori_loop(0, ep_count - minor, sum_step, 0)
+
+    y_copy = remote(ys_buf, yr_buf, ry_s, ry_r, mate_y)
+    gather_sum(z, z * minor + 1 - y)
+    ys_buf[...] = acc[...].astype(jnp.bfloat16)
+    y_copy.start()
+    gather_sum(z, e)
+    y_copy.wait_recv()
+    final = acc[...] + yr_buf[...].astype(jnp.float32)
+    f_copy = remote(fs_buf, fr_buf, f_s, f_r, mate_x)
+    fs_buf[...] = final[:, quarter:].astype(jnp.bfloat16)
+    f_copy.start()
+    out_ref[:, :split] = (final[:, :split] + sh_out[:, :split]).astype(jnp.bfloat16)
+    f_copy.wait_recv()
+    out_ref[:, split:] = (
+        final[:, split:quarter] + fr_buf[...].astype(jnp.float32) + sh_out[:, split:]
+    ).astype(jnp.bfloat16)
+
+    f_copy.wait_send()
+    y_copy.wait_send()
+    for copy in line(e, y_s, mate_y):
+        copy.wait_send()
+    for k in range(1, ep_count):
+        wt_copy(k, None, lax.rem(e + k, ep_count)).wait_send()
+    for k in range(1, tp_count):
+        sh_copy(k, t, lax.rem(t + k, tp_count)).wait_send()
+
+    def drain(i, carry):
+        p, g = slot_group(i)
+
+        @pl.when((p <= z) & (z < major - 1))
+        def _():
+            for copy in line(g, u_s, z_up):
+                copy.wait_send()
+
+        @pl.when((p >= z) & (z > 0))
+        def _():
+            for copy in line(g, d_s, z_down):
+                copy.wait_send()
+
+        @pl.when(i > 0)
+        def _():
+            x_copy(g).wait_send()
+            for copy in c_copies(g, c):
+                copy.wait_send()
+
+        for k in range(2):
+            yc_copy(g, k).wait_send()
+        rx_copy(g).wait_send()
+
+        @pl.when(p != z)
+        def _():
+            rz_copy(g, 0, z_up).wait_send()
+
+        return carry
+
+    lax.fori_loop(0, total, drain, 0)
+
+
+def dense_exchange(
+    tokens, norm_gain, expert_ids, route_weights, expert_gate, expert_up, expert_down,
+    shared_gate, shared_up, shared_down,
+):
+    ep_count = lax.axis_size("ep")
+    tp_count = lax.axis_size("tp")
+    minor = 1 << (ep_count.bit_length() - 1) // 2
+    rows, width = tokens.shape
+    quarter = width // tp_count
+    split = quarter * 3 // 4 // LANES * LANES
+    expert_count = ep_count * tp_count // 2
+    wide = quarter + quarter - split
+    expert_iota = jnp.arange(expert_count, dtype=jnp.int32)
+    table = jnp.sum(
+        jnp.where(
+            expert_ids[None, :, :] == expert_iota[:, None, None], route_weights[None, :, :], 0.0
+        ),
+        axis=2,
+    )
+    ff = expert_gate.shape[2]
+    share = shared_gate.shape[1]
+    bf16, f32 = jnp.bfloat16, jnp.float32
+    dma = pltpu.SemaphoreType.DMA
+    vmem = pl.BlockSpec(memory_space=pltpu.VMEM)
+    anywhere = pl.BlockSpec(memory_space=pl.ANY)
+    n = ep_count
+    return pl.pallas_call(
+        functools.partial(dense_kernel, ep_count, tp_count, minor, split),
+        out_shape=jax.ShapeDtypeStruct((rows, quarter), bf16),
+        in_specs=[vmem] * 3 + [anywhere] * 6,
+        out_specs=vmem,
+        scratch_shapes=[
+            pltpu.VMEM((n, tp_count, rows, quarter), bf16),
+            pltpu.VMEM((n, tp_count, rows, quarter), bf16),
+            pltpu.VMEM((n, 2, rows, quarter), bf16),
+            pltpu.VMEM((n, rows, split), bf16),
+            pltpu.VMEM((n, rows, split), bf16),
+            pltpu.VMEM((n, rows, wide), bf16),
+            pltpu.VMEM((2, n, rows, wide), bf16),
+            pltpu.VMEM((rows, wide), bf16),
+            pltpu.VMEM((rows, wide), bf16),
+            pltpu.VMEM((rows, quarter - split), bf16),
+            pltpu.VMEM((rows, quarter - split), bf16),
+            pltpu.VMEM((rows, wide), f32),
+            pltpu.VMEM((n, expert_count, rows), f32),
+            pltpu.VMEM((tp_count, rows, share), bf16),
+            pltpu.VMEM((rows, quarter), f32),
+            pltpu.VMEM((width, ff), bf16),
+            pltpu.VMEM((width, ff), bf16),
+            pltpu.VMEM((ff, width), bf16),
+            pltpu.VMEM((width, share), bf16),
+            pltpu.VMEM((width, share), bf16),
+            pltpu.VMEM((share * tp_count, quarter), bf16),
+            dma((6,)), dma((n,)), dma((n,)), dma((tp_count,)), dma((tp_count,)),
+            dma((n, 2)), dma((n, 2)), dma((n, 2)), dma((n, 2)),
+            dma((n,)), dma((n,)), dma((n, 3)), dma((n, 3)),
+            dma((n, 2)), dma((n, 2)), dma((n,)), dma((n,)),
+            dma((n,)), dma((2, n)), dma, dma, dma, dma,
+        ],
+        compiler_params=pltpu.CompilerParams(
+            collective_id=0, has_side_effects=True, vmem_limit_bytes=60 << 20
+        ),
+        name="dense_moe",
+    )(
+        tokens, norm_gain.reshape(1, width), table, expert_gate[0], expert_up[0], expert_down[0],
+        shared_gate, shared_up, shared_down,
+    )
+
+
+def local(tokens, *rest):
+    ep_count = lax.axis_size("ep")
+    pair_count = lax.axis_size("tp") // 2
+    dense_bytes = 4 * ep_count * tokens.size * tokens.dtype.itemsize
+    minor = 1 << (ep_count.bit_length() - 1) // 2
+    if pair_count == 2 and minor == 2 and dense_bytes <= 24 << 20:
+        return dense_exchange(tokens, *rest)
+    return routed_exchange(tokens, *rest)
+
+
 def solution(mesh):
     return jax.shard_map(
         local,

time: 198 us -> 95.1 us (0.48)
  waiting for transfers between devices: 127 us -> 0 us
  Pallas kernels: 0 us -> 91.3 us
  matrix products: 16.2 us -> 0 us
  between operations: 13.6 us -> 0.01 us
  starting transfers between devices: 11.1 us -> 0 us
  local copies, waits for them, and re-layouts: 12.8 us -> 2.25 us
  other arithmetic: 11.6 us -> 1.3 us
  blocking collectives: 5.45 us -> 0 us
    all_to_all x2 -> x0, waiting for transfers between devices: 108 us -> none  [the longest x1 70.8 us: local(): lax.all_to_all(buffer, 'ep', split_axis=0, concat_axis=0, tiled=True)]
    pallas_call x0 -> x1, Pallas kernels: none -> 91.3 us  [dense_exchange(): pl.pallas_call(functools.partial(dense_kernel, ep_count, tp_count, minor,...]
    dot_general x7 -> x0, matrix products: 16.2 us -> none  [the longest x1 7.39 us: local(): jnp.dot(hidden, down_local, preferred_element_type=jnp.float32)]
    reduce_scatter x1 -> x0, waiting for transfers between devices: 15.6 us -> none  [local(): lax.psum_scatter(partial_routed, 'tp', scatter_dimension=1, tiled=True)]
    all_to_all x2 -> x0, starting transfers between devices: 11.1 us -> none  [the longest x1 7.44 us: local(): lax.all_to_all(buffer, 'ep', split_axis=0, concat_axis=0, tiled=True)]
    gather x6 -> x0, local copies, waits for them, and re-layouts: 9.85 us -> none  [the longest x5 5.56 us: local(): jnp.take_along_axis(prefix, expert_ids, axis=1).astype(jnp.int32)]
    all_gather x1 -> x0, blocking collectives: 5.45 us -> none  [local(): lax.all_gather(shared_act, 'tp', axis=1, tiled=True)]
    convert_element_type x3 -> x0, other arithmetic: 4.98 us -> none  [the longest x1 3.15 us: local(): (kept_part.astype(jnp.float32) + partner_part.astype(jnp.float32)).astype...]
  transfers between devices with their start and end apart: 4 -> 0, of which waited for: 4 -> 0; matrix products, arithmetic and copies ran while one was open for 2% -> 0% of each run, Pallas kernels for 0% -> 0%
where the time goes in v1:
time: 95.1 us; the launch traced here: 94.9 us
  Pallas kernels  91.3 us (96%)
  local copies, waits for them, and re-layouts  2.25 us (2%)
  other arithmetic  1.3 us (1%)
    pallas_call x1, Pallas kernels, dense_exchange(): pl.pallas_call(functools.partial(dense_kernel, ep_count, tp_count, minor,...  91.3 us
    unnamed x3, local copies, waits for them, and re-layouts  2.25 us

profile of v1, /device:TPU:0, one launch (start us, length us, event | category | flops | bytes accessed | tf_op | source)
XLA Modules:
  0.0 94.9 jit_solution(13938791809287460774)
XLA Ops:
  0.0 0.0 copy-start
  0.0 0.7 copy-done
  0.7 1.3 %select_reduce_fusion.wt_ref = f32[16,128]{1,0:T(8,128)} fusion(f32[128,6]{0,1:T(8,128)S(1)} %copy-done, s32[128,6]{0,1:T(8,128)} %param.12), kind=kLoop, calls=%fused_computation | loop fusion | flops 34816 | bytes 14336 | tf_op jit(solution)/shard_map/reduce_sum | solution.py:465
  2.0 91.3 %dense_moe.1 = bf16[128,512]{1,0:T(8,128)(2,1)} custom-call(bf16[128,2048]{1,0:T(8,128)(2,1)} %tok_ref.1, f32[1,2048]{1,0:T(1,128)} %bitcast.7, f32[16,128]{1,0:T(8,128)} %select_reduce_fusion.wt_ref, bf16[2048,256]{1,0:T(8,128)(2,1)} %bitcast.4, bf16[2048,256]{1,0:T(8,128)(2,1)} %bitcast.5, bf16[256,2048]{1,0:T(8,128)(2,1)} %bitcast.6, ...), custom_call_target="tpu_custom_call" | custom-call | tf_op jit(solution)/shard_map/dense_moe/pallas_call | solution.py:478
  93.3 1.6 %copy.14 = bf16[128,512]{1,0:T(8,128)(2,1)} copy(bf16[128,512]{1,0:T(8,128)(2,1)} %dense_moe.1) | data formatting | bytes 262144
Async XLA Ops:
  0.0 0.7 copy-start

commit v2 on v1

--- a/solution.py
+++ b/solution.py
@@ -125,10 +125,12 @@
     ep_count, tp_count, minor, split,
     tok_ref, gain_ref, wt_ref, gate_hbm, up_hbm, down_hbm, sg_hbm, su_hbm, sd_hbm,
     out_ref,
-    x_buf, y_buf, c_buf, xs_buf, xr_buf, zs_buf, zr_buf, ys_buf, yr_buf, fs_buf, fr_buf,
+    x_buf, y_buf, c_buf, xs_buf, xr_buf, ysa_buf, yra_buf, zsa_buf, zra_buf, zs_buf, zr_buf,
+    ys_buf, yr_buf, fs_buf, fr_buf,
     acc, wt_all, sh_all, sh_out, gate, up, down, sg, su, sd,
     load_sem, wt_s, wt_r, sh_s, sh_r, y_s, u_s, d_s, z_r, x_s, x_r, c_s, c_r,
-    yc_s, yc_r, rx_s, rx_r, rz_s, rz_r, ry_s, ry_r, f_s, f_r,
+    ya_s, ya_r, yc_s, yc_r, rx_s, rx_r, rya_s, rya_r, rza_s, rza_r, rz_s, rz_r, ry_s, ry_r,
+    f_s, f_r,
 ):
     major = ep_count // minor
     rows = tok_ref.shape[0]
@@ -187,17 +189,23 @@
         dst = wt_all.at[e if slot is None else slot]
         return remote(src, dst, wt_s.at[k], wt_r.at[k], {"ep": who})
 
-    def main_of(g):
-        return x_buf.at[g, t]
-
-    def rest_of(g):
-        return x_buf.at[g, t2, :, rest_cols]
-
-    def line(g, s, who):
+    def head_of(g, q):
+        return x_buf.at[g, q, :, head_cols]
+
+    def rest_of(g, q):
+        return x_buf.at[g, q, :, rest_cols]
+
+    def line_head(g, s, who):
+        return (remote(head_of(g, t), head_of(g, t), s.at[g, 0], z_r.at[g, 0], who),)
+
+    def line_rest(g, s, who):
         return (
-            remote(main_of(g), main_of(g), s.at[g, 0], z_r.at[g, 0], who),
-            remote(rest_of(g), rest_of(g), s.at[g, 1], z_r.at[g, 1], who),
+            remote(rest_of(g, t), rest_of(g, t), s.at[g, 1], z_r.at[g, 1], who),
+            remote(rest_of(g, t2), rest_of(g, t2), s.at[g, 2], z_r.at[g, 2], who),
         )
+
+    def y_copy_head(g):
+        return remote(head_of(g, t), head_of(g, t), ya_s.at[g], ya_r.at[g], mate_y)
 
     def x_copy(g):
         ref = x_buf.at[g, t, :, head_cols]
@@ -209,7 +217,7 @@
 
     def c_copies(g, lane):
         main, other = 2 * xi + lane, 2 * (1 - xi) + lane
-        refs = (x_buf.at[g, main], x_buf.at[g, other, :, rest_cols], x_buf.at[g, other, :, head_cols])
+        refs = (head_of(g, main), rest_of(g, main), rest_of(g, other), head_of(g, other))
         return [remote(r, r, c_s.at[g, i], c_r.at[g, i], mate_c) for i, r in enumerate(refs)]
 
     def order(j):
@@ -224,23 +232,25 @@
         yy = jnp.where(i % 2 == 0, y, 1 - y)
         return p, p * minor + yy
 
-    def forward(p, g):
+    def forward(p, g, pieces):
         @pl.when((p <= z) & (z < major - 1))
         def _():
-            for copy in line(g, u_s, z_up):
+            for copy in pieces(g, u_s, z_up):
                 copy.start()
 
         @pl.when((p >= z) & (z > 0))
         def _():
-            for copy in line(g, d_s, z_down):
+            for copy in pieces(g, d_s, z_down):
                 copy.start()
 
-    for copy in line(e, y_s, mate_y):
+    for copy in line_rest(e, y_s, mate_y):
         copy.start()
+    forward(z, e, line_head)
+    y_copy_head(e).start()
     for k in range(1, ep_count):
         wt_copy(k, None, lax.rem(e + k, ep_count)).start()
     wt_all[e] = wt_ref[...]
-    forward(z, e)
+    forward(z, e, line_rest)
 
     loads[0].wait()
     loads[1].wait()
@@ -293,28 +303,53 @@
     def rx_copy(g):
         return remote(xs_buf.at[g], xr_buf.at[g], rx_s.at[g], rx_r.at[g], mate_x)
 
+    def rya_copy(p):
+        return remote(ysa_buf.at[p], yra_buf.at[p], rya_s.at[p], rya_r.at[p], mate_y)
+
     total = ep_count
+
+    def head_sum(g):
+        return (
+            y_buf[g, t, :, head_cols].astype(jnp.float32)
+            + c_buf[g, xi, :, head_cols].astype(jnp.float32)
+            + xr_buf[g].astype(jnp.float32)
+        )
 
     def main_step(i, carry):
         @pl.when((i >= 1) & (i < total))
         def _():
             p, g = slot_group(i)
-            for copy in line(g, u_s, z_up):
+            ours = c_copies(g, c)
+
+            @pl.when(i % 2 == 0)
+            def _():
+                line_head(g, u_s, z_up)[0].wait_recv()
+                forward(p, g, line_head)
+                y_copy_head(g).start()
+                x_copy(g).start()
+                ours[0].start()
+
+            for copy in line_rest(g, u_s, z_up):
                 copy.wait_recv()
-            forward(p, g)
+            forward(p, g, line_rest)
+            ours[1].start()
+            ours[2].start()
+
+        @pl.when((i >= 2) & (i <= total) & (i % 2 == 0))
+        def _():
+            _, g = slot_group(i - 1)
+            y_copy_head(g).wait_recv()
             x_copy(g).start()
-            ours = c_copies(g, c)
-            ours[0].start()
-            ours[1].start()
-
-        @pl.when((i >= 1) & (i <= total))
-        def _():
-            _, g = slot_group(i - 1)
-
-            @pl.when(i >= 2)
+            c_copies(g, c)[0].start()
+
+        @pl.when((i >= 2) & (i <= total + 1))
+        def _():
+            _, g = slot_group(i - 2)
+
+            @pl.when(i >= 3)
             def _():
                 x_arrival(g).wait_recv()
-                c_copies(g, c)[2].start()
+                c_copies(g, c)[3].start()
                 for copy in c_copies(g, 1 - c):
                     copy.wait_recv()
 
@@ -322,9 +357,9 @@
             for k in range(2):
                 yc_copy(g, k).start()
 
-        @pl.when(i >= 2)
-        def _():
-            _, g = slot_group(i - 2)
+        @pl.when((i >= 3) & (i <= total + 2))
+        def _():
+            _, g = slot_group(i - 3)
             for k in range(2):
                 yc_copy(g, k).wait_recv()
             xs_buf[g] = (
@@ -333,9 +368,16 @@
             ).astype(jnp.bfloat16)
             rx_copy(g).start()
 
+        @pl.when((i >= 5) & (i % 2 == 1))
+        def _():
+            p, g = slot_group(i - 4)
+            rx_copy(g).wait_recv()
+            ysa_buf[p] = head_sum(g).astype(jnp.bfloat16)
+            rya_copy(p).start()
+
         return carry
 
-    lax.fori_loop(0, total + 2, main_step, 0)
+    lax.fori_loop(0, total + 4, main_step, 0)
 
     loads[5].wait()
     for k in range(1, tp_count):
@@ -351,11 +393,13 @@
     def rz_copy(g, lane, who):
         return remote(zs_buf.at[g], zr_buf.at[lane, g], rz_s.at[g], rz_r.at[lane, g], who)
 
-    def gather_sum(p, g):
-        rx_copy(g).wait_recv()
-        mine = y_buf[g, t].astype(jnp.float32) + c_buf[g, xi].astype(jnp.float32)
-        acc[:, :split] = mine[:, :split] + xr_buf[g].astype(jnp.float32)
-        acc[:, split:quarter] = mine[:, split:]
+    def rza_copy(p, lane, who):
+        return remote(zsa_buf.at[p], zra_buf.at[lane, p], rza_s.at[p], rza_r.at[lane, p], who)
+
+    def sum_rest(p, g):
+        acc[:, split:quarter] = y_buf[g, t, :, rest_cols].astype(jnp.float32) + c_buf[
+            g, xi, :, rest_cols
+        ].astype(jnp.float32)
         acc[:, quarter:] = y_buf[g, t2, :, rest_cols].astype(jnp.float32) + c_buf[
             g, 1 - xi, :, rest_cols
         ].astype(jnp.float32)
@@ -363,42 +407,64 @@
         @pl.when((p >= z) & (z > 0))
         def _():
             rz_copy(g, 0, z_up).wait_recv()
-            acc[...] += zr_buf[0, g].astype(jnp.float32)
+            acc[:, split:] += zr_buf[0, g].astype(jnp.float32)
 
         @pl.when((p <= z) & (z < major - 1))
         def _():
             rz_copy(g, 1, z_up).wait_recv()
-            acc[...] += zr_buf[1, g].astype(jnp.float32)
-
-    def sum_step(i, carry):
-        q = i // 2
+            acc[:, split:] += zr_buf[1, g].astype(jnp.float32)
+
+    def sum_head(p, g):
+        rx_copy(g).wait_recv()
+        rya_copy(p).wait_recv()
+        acc[:, :split] = head_sum(g) + yra_buf[p].astype(jnp.float32)
+
+        @pl.when((p >= z) & (z > 0))
+        def _():
+            rza_copy(p, 0, z_up).wait_recv()
+            acc[:, :split] += zra_buf[0, p].astype(jnp.float32)
+
+        @pl.when((p <= z) & (z < major - 1))
+        def _():
+            rza_copy(p, 1, z_up).wait_recv()
+            acc[:, :split] += zra_buf[1, p].astype(jnp.float32)
+
+    def sum_step(q, carry):
         ups = major - 1 - z
         low = jnp.where(q < ups, z + 1 + q, z - 1 - (q - ups))
         high = jnp.where(q < z, z - 1 - q, z + 1 + (q - z))
         p = jnp.where(2 * z < major, low, high)
-        g = p * minor + jnp.where(i % 2 == 0, y, 1 - y)
-        gather_sum(p, g)
-        zs_buf[g] = acc[...].astype(jnp.bfloat16)
-
-        @pl.when(p > z)
-        def _():
-            rz_copy(g, 0, z_up).start()
-
-        @pl.when(p < z)
-        def _():
-            rz_copy(g, 1, z_down).start()
-
+
+        def send(copy, key):
+            @pl.when(p > z)
+            def _():
+                copy(key, 0, z_up).start()
+
+            @pl.when(p < z)
+            def _():
+                copy(key, 1, z_down).start()
+
+        for yy in (1 - y, y):
+            g = p * minor + yy
+            sum_rest(p, g)
+            zs_buf[g] = acc[:, split:].astype(jnp.bfloat16)
+            send(rz_copy, g)
+        sum_head(p, p * minor + y)
+        zsa_buf[p] = acc[:, :split].astype(jnp.bfloat16)
+        send(rza_copy, p)
         return carry
 
-    lax.fori_loop(0, ep_count - minor, sum_step, 0)
+    lax.fori_loop(0, major - 1, sum_step, 0)
 
     y_copy = remote(ys_buf, yr_buf, ry_s, ry_r, mate_y)
-    gather_sum(z, z * minor + 1 - y)
-    ys_buf[...] = acc[...].astype(jnp.bfloat16)
+    sum_rest(z, z * minor + 1 - y)
+    ys_buf[...] = acc[:, split:].astype(jnp.bfloat16)
     y_copy.start()
-    gather_sum(z, e)
+    sum_rest(z, e)
+    sum_head(z, e)
     y_copy.wait_recv()
-    final = acc[...] + yr_buf[...].astype(jnp.float32)
+    acc[:, split:] += yr_buf[...].astype(jnp.float32)
+    final = acc[...]
     f_copy = remote(fs_buf, fr_buf, f_s, f_r, mate_x)
     fs_buf[...] = final[:, quarter:].astype(jnp.bfloat16)
     f_copy.start()
@@ -410,7 +476,7 @@
 
     f_copy.wait_send()
     y_copy.wait_send()
-    for copy in line(e, y_s, mate_y):
+    for copy in line_rest(e, y_s, mate_y):
         copy.wait_send()
     for k in range(1, ep_count):
         wt_copy(k, None, lax.rem(e + k, ep_count)).wait_send()
@@ -420,15 +486,31 @@
     def drain(i, carry):
         p, g = slot_group(i)
 
-        @pl.when((p <= z) & (z < major - 1))
-        def _():
-            for copy in line(g, u_s, z_up):
-                copy.wait_send()
-
-        @pl.when((p >= z) & (z > 0))
-        def _():
-            for copy in line(g, d_s, z_down):
-                copy.wait_send()
+        def sent(pieces):
+            @pl.when((p <= z) & (z < major - 1))
+            def _():
+                for copy in pieces(g, u_s, z_up):
+                    copy.wait_send()
+
+            @pl.when((p >= z) & (z > 0))
+            def _():
+                for copy in pieces(g, d_s, z_down):
+                    copy.wait_send()
+
+        sent(line_rest)
+
+        @pl.when(i % 2 == 0)
+        def _():
+            sent(line_head)
+            y_copy_head(g).wait_send()
+
+            @pl.when(p != z)
+            def _():
+                rza_copy(p, 0, z_up).wait_send()
+
+        @pl.when(i % 2 == 1)
+        def _():
+            rya_copy(p).wait_send()
 
         @pl.when(i > 0)
         def _():
@@ -475,6 +557,7 @@
     vmem = pl.BlockSpec(memory_space=pltpu.VMEM)
     anywhere = pl.BlockSpec(memory_space=pl.ANY)
     n = ep_count
+    major = n // minor
     return pl.pallas_call(
         functools.partial(dense_kernel, ep_count, tp_count, minor, split),
         out_shape=jax.ShapeDtypeStruct((rows, quarter), bf16),
@@ -486,10 +569,14 @@
             pltpu.VMEM((n, 2, rows, quarter), bf16),
             pltpu.VMEM((n, rows, split), bf16),
             pltpu.VMEM((n, rows, split), bf16),
-            pltpu.VMEM((n, rows, wide), bf16),
-            pltpu.VMEM((2, n, rows, wide), bf16),
-            pltpu.VMEM((rows, wide), bf16),
-            pltpu.VMEM((rows, wide), bf16),
+            pltpu.VMEM((major, rows, split), bf16),
+            pltpu.VMEM((major, rows, split), bf16),
+            pltpu.VMEM((major, rows, split), bf16),
+            pltpu.VMEM((2, major, rows, split), bf16),
+            pltpu.VMEM((n, rows, wide - split), bf16),
+            pltpu.VMEM((2, n, rows, wide - split), bf16),
+            pltpu.VMEM((rows, wide - split), bf16),
+            pltpu.VMEM((rows, wide - split), bf16),
             pltpu.VMEM((rows, quarter - split), bf16),
             pltpu.VMEM((rows, quarter - split), bf16),
             pltpu.VMEM((rows, wide), f32),
@@ -503,10 +590,10 @@
             pltpu.VMEM((width, share), bf16),
             pltpu.VMEM((share * tp_count, quarter), bf16),
             dma((6,)), dma((n,)), dma((n,)), dma((tp_count,)), dma((tp_count,)),
-            dma((n, 2)), dma((n, 2)), dma((n, 2)), dma((n, 2)),
-            dma((n,)), dma((n,)), dma((n, 3)), dma((n, 3)),
-            dma((n, 2)), dma((n, 2)), dma((n,)), dma((n,)),
-            dma((n,)), dma((2, n)), dma, dma, dma, dma,
+            dma((n, 3)), dma((n, 3)), dma((n, 3)), dma((n, 3)),
+            dma((n,)), dma((n,)), dma((n, 4)), dma((n, 4)), dma((n,)), dma((n,)),
+            dma((n, 2)), dma((n, 2)), dma((n,)), dma((n,)), dma((major,)), dma((major,)),
+            dma((major,)), dma((2, major)), dma((n,)), dma((2, n)), dma, dma, dma, dma,
         ],
         compiler_params=pltpu.CompilerParams(
             collective_id=0, has_side_effects=True, vmem_limit_bytes=60 << 20

time: 95.1 us -> 90 us (0.946)
  Pallas kernels: 91.3 us -> 86.3 us
    pallas_call x1, Pallas kernels: 91.3 us -> 86.3 us  [dense_exchange(): pl.pallas_call(functools.partial(dense_kernel, ep_count, tp_count, minor,...]
where the time goes in v2:
time: 90 us; the launch traced here: 89.8 us
  Pallas kernels  86.3 us (96%)
  local copies, waits for them, and re-layouts  2.25 us (2%)
  other arithmetic  1.3 us (1%)
    pallas_call x1, Pallas kernels, dense_exchange(): pl.pallas_call(functools.partial(dense_kernel, ep_count, tp_count, minor,...  86.3 us
    unnamed x3, local copies, waits for them, and re-layouts  2.25 us

profile of v2, /device:TPU:0, one launch (start us, length us, event | category | flops | bytes accessed | tf_op | source)
XLA Modules:
  0.0 89.8 jit_solution(5236334778415063888)
XLA Ops:
  0.0 0.0 copy-start
  0.0 0.7 copy-done
  0.7 1.3 %select_reduce_fusion.wt_ref = f32[16,128]{1,0:T(8,128)} fusion(f32[128,6]{0,1:T(8,128)S(1)} %copy-done, s32[128,6]{0,1:T(8,128)} %param.12), kind=kLoop, calls=%fused_computation | loop fusion | flops 34816 | bytes 14336 | tf_op jit(solution)/shard_map/reduce_sum | solution.py:547
  2.0 86.3 %dense_moe.1 = bf16[128,512]{1,0:T(8,128)(2,1)} custom-call(bf16[128,2048]{1,0:T(8,128)(2,1)} %tok_ref.1, f32[1,2048]{1,0:T(1,128)} %bitcast.7, f32[16,128]{1,0:T(8,128)} %select_reduce_fusion.wt_ref, bf16[2048,256]{1,0:T(8,128)(2,1)} %bitcast.4, bf16[2048,256]{1,0:T(8,128)(2,1)} %bitcast.5, bf16[256,2048]{1,0:T(8,128)(2,1)} %bitcast.6, ...), custom_call_target="tpu_custom_call" | custom-call | tf_op jit(solution)/shard_map/dense_moe/pallas_call | solution.py:561
  88.3 1.6 %copy.14 = bf16[128,512]{1,0:T(8,128)(2,1)} copy(bf16[128,512]{1,0:T(8,128)(2,1)} %dense_moe.1) | data formatting | bytes 262144
Async XLA Ops:
  0.0 0.7 copy-start

commit v3 on v2

--- a/solution.py
+++ b/solution.py
@@ -342,14 +342,18 @@
             x_copy(g).start()
             c_copies(g, c)[0].start()
 
-        @pl.when((i >= 2) & (i <= total + 1))
-        def _():
-            _, g = slot_group(i - 2)
-
-            @pl.when(i >= 3)
+        @pl.when((i >= 4) & (i <= total + 2))
+        def _():
+            _, g = slot_group(i - 3)
+            x_arrival(g).wait_recv()
+            c_copies(g, c)[3].start()
+
+        @pl.when((i >= 4) & (i <= total + 3))
+        def _():
+            _, g = slot_group(i - 4)
+
+            @pl.when(i >= 5)
             def _():
-                x_arrival(g).wait_recv()
-                c_copies(g, c)[3].start()
                 for copy in c_copies(g, 1 - c):
                     copy.wait_recv()
 
@@ -357,9 +361,9 @@
             for k in range(2):
                 yc_copy(g, k).start()
 
-        @pl.when((i >= 3) & (i <= total + 2))
-        def _():
-            _, g = slot_group(i - 3)
+        @pl.when((i >= 5) & (i <= total + 4))
+        def _():
+            _, g = slot_group(i - 5)
             for k in range(2):
                 yc_copy(g, k).wait_recv()
             xs_buf[g] = (
@@ -368,16 +372,16 @@
             ).astype(jnp.bfloat16)
             rx_copy(g).start()
 
-        @pl.when((i >= 5) & (i % 2 == 1))
-        def _():
-            p, g = slot_group(i - 4)
+        @pl.when((i >= 8) & (i % 2 == 0))
+        def _():
+            p, g = slot_group(i - 7)
             rx_copy(g).wait_recv()
             ysa_buf[p] = head_sum(g).astype(jnp.bfloat16)
             rya_copy(p).start()
 
         return carry
 
-    lax.fori_loop(0, total + 4, main_step, 0)
+    lax.fori_loop(0, total + 7, main_step, 0)
 
     loads[5].wait()
     for k in range(1, tp_count):

time: 90 us -> 84.2 us (0.936)
  Pallas kernels: 86.3 us -> 80.5 us
    pallas_call x1, Pallas kernels: 86.3 us -> 80.5 us  [dense_exchange(): pl.pallas_call(functools.partial(dense_kernel, ep_count, tp_count, minor,...]
where the time goes in v3:
time: 84.2 us; the launch traced here: 84 us
  Pallas kernels  80.5 us (96%)
  local copies, waits for them, and re-layouts  2.25 us (3%)
  other arithmetic  1.3 us (2%)
    pallas_call x1, Pallas kernels, dense_exchange(): pl.pallas_call(functools.partial(dense_kernel, ep_count, tp_count, minor,...  80.5 us
    unnamed x3, local copies, waits for them, and re-layouts  2.25 us

profile of v3, /device:TPU:0, one launch (start us, length us, event | category | flops | bytes accessed | tf_op | source)
XLA Modules:
  0.0 84.0 jit_solution(7822648755241324073)
XLA Ops:
  0.0 0.0 copy-start
  0.0 0.7 copy-done
  0.7 1.3 %select_reduce_fusion.wt_ref = f32[16,128]{1,0:T(8,128)} fusion(f32[128,6]{0,1:T(8,128)S(1)} %copy-done, s32[128,6]{0,1:T(8,128)} %param.12), kind=kLoop, calls=%fused_computation | loop fusion | flops 34816 | bytes 14336 | tf_op jit(solution)/shard_map/reduce_sum | solution.py:551
  2.0 80.5 %dense_moe.1 = bf16[128,512]{1,0:T(8,128)(2,1)} custom-call(bf16[128,2048]{1,0:T(8,128)(2,1)} %tok_ref.1, f32[1,2048]{1,0:T(1,128)} %bitcast.7, f32[16,128]{1,0:T(8,128)} %select_reduce_fusion.wt_ref, bf16[2048,256]{1,0:T(8,128)(2,1)} %bitcast.4, bf16[2048,256]{1,0:T(8,128)(2,1)} %bitcast.5, bf16[256,2048]{1,0:T(8,128)(2,1)} %bitcast.6, ...), custom_call_target="tpu_custom_call" | custom-call | tf_op jit(solution)/shard_map/dense_moe/pallas_call | solution.py:565
  82.5 1.6 %copy.14 = bf16[128,512]{1,0:T(8,128)(2,1)} copy(bf16[128,512]{1,0:T(8,128)(2,1)} %dense_moe.1) | data formatting | bytes 262144
Async XLA Ops:
  0.0 0.7 copy-start
